TPU v7x, 32 devices: a whole 2x2x4 slice. The times are simulated.
32 devices in a mesh: ep: 8 (over z, x), tp: 4 (over y, core).
Axes of the slice: x: 2, y: 2, z: 4, core: 2. Of those that a mesh axis runs over, the one named last changes fastest.
Arguments:
- q_in: bfloat16 [4096, 1024], P('ep', 'tp'), may hold values from -6 to 6
- k_in: bfloat16 [4096, 256], P('ep'), may hold values from -6 to 6
- v_in: bfloat16 [4096, 256], P('ep'), may hold values from -6 to 6
- q_gain: float32 [64], replicated, may hold values from 0.1 to 1.9
- k_gain: float32 [64], replicated, may hold values from 0.1 to 1.9
- w_out: bfloat16 [1024, 2048], P('tp'), may hold values from -0.1875 to 0.1875
- post_gain: float32 [2048], replicated, may hold values from 0.1 to 1.9
- moe_in: bfloat16 [1024, 2048], P('ep'), may hold values from -6 to 6
- routes: int32 [1024, 2], P('ep'), may hold values from 0 to 7, all different within a row; in each aligned block of 128 rows (0 to 127, 128 to 255, ...) at most 48 rows name the same one
- route_logits: float32 [1024, 2], P('ep'), may hold values from -6 to 6
- pre_gain: float32 [2048], replicated, may hold values from 0.1 to 1.9
- w_gate: bfloat16 [8, 2048, 4096], P('ep', None, 'tp'), may hold values from -0.125 to 0.125
- w_up: bfloat16 [8, 2048, 4096], P('ep', None, 'tp'), may hold values from -0.125 to 0.125
- w_down: bfloat16 [8, 4096, 2048], P('ep', 'tp'), may hold values from -0.125 to 0.125
Outputs:
- attn_out: bfloat16 [4096, 2048], P(('ep', 'tp'))
- moe_out: bfloat16 [1024, 2048], P('ep', 'tp')
Inputs may be any that keep to these rules, and one draw needn't show every extreme that they name: `routes`: each row names 2 different experts. Among the rows of one index of ep no expert is named by more than 48 rows, a bound that some block reaches of them.
All inputs are finite; a program needn't handle non-finite values.
Results may differ from a plain program's by a relative error of at most 0.018.
Values may be sent and summed in bfloat16 or wider, within the bound.
A program may use at most 64 MiB of HBM per device.

v0:
```python
import jax
import jax.numpy as jnp
from jax import lax
from jax.sharding import PartitionSpec as P

GRID_W = 128
EPSILON = 1e-06
ROPE_BASE = 10000.0


def head_norm(values, gain):
    return values * lax.rsqrt(jnp.mean(values * values, axis=-1, keepdims=True) + EPSILON) * gain


def rotate_half(values, angles):
    quarter = angles.shape[-1]
    first_part = values[..., :quarter]
    second_part = values[..., quarter:]
    cosine = jnp.cos(angles)[:, None, :]
    sine_part = jnp.sin(angles)[:, None, :]
    return jnp.concatenate(
        [
            first_part * cosine - second_part * sine_part,
            second_part * cosine + first_part * sine_part,
        ],
        axis=-1,
    )


def grid_rotary(values, offset):
    row_count = values.shape[0]
    head_width = values.shape[-1]
    quarter = head_width // 4
    half_width = head_width // 2
    position = offset + jnp.arange(row_count, dtype=jnp.int32)
    grid_row = (position // GRID_W).astype(jnp.float32)
    grid_col = (position % GRID_W).astype(jnp.float32)
    inverse = ROPE_BASE ** (-jnp.arange(quarter, dtype=jnp.float32) / quarter)
    return jnp.concatenate(
        [
            rotate_half(values[..., :half_width], grid_row[:, None] * inverse[None, :]),
            rotate_half(values[..., half_width:], grid_col[:, None] * inverse[None, :]),
        ],
        axis=-1,
    )


def slot_table(route_rows, expert_count, capacity):
    token_count, top_count = route_rows.shape
    flat_routes = route_rows.reshape(-1)
    one_hot = (flat_routes[:, None] == jnp.arange(expert_count, dtype=jnp.int32)[None, :]).astype(
        jnp.int32
    )
    ranked = jnp.sum((jnp.cumsum(one_hot, axis=0) - 1) * one_hot, axis=1)
    placed = flat_routes * capacity + ranked
    slot_owner = jnp.full((expert_count * capacity,), token_count * top_count, dtype=jnp.int32)
    slot_owner = slot_owner.at[placed].set(jnp.arange(token_count * top_count, dtype=jnp.int32))
    return (slot_owner, placed)


def mixer_half(q_in, k_in, v_in, q_gain, k_gain, w_out, post_gain):
    head_size = q_gain.shape[0]
    row_count = q_in.shape[0]
    local_heads = q_in.shape[1] // head_size
    kv_count = k_in.shape[1] // head_size
    tp_count = lax.axis_size("tp")
    repeat = local_heads * tp_count // kv_count
    offset = lax.axis_index("ep") * row_count
    queries = head_norm(q_in.astype(jnp.float32).reshape(row_count, local_heads, head_size), q_gain)
    queries = grid_rotary(queries, offset).astype(jnp.bfloat16)
    query_rows = jnp.transpose(queries, (1, 0, 2)).reshape(local_heads * row_count, head_size)
    kv_index = lax.axis_index("tp") * local_heads // repeat
    own_keys = lax.dynamic_slice_in_dim(k_in, kv_index * head_size, head_size, 1)
    own_values = lax.dynamic_slice_in_dim(v_in, kv_index * head_size, head_size, 1)
    own_keys = head_norm(own_keys.astype(jnp.float32)[:, None, :], k_gain)
    own_keys = grid_rotary(own_keys, offset)[:, 0, :].astype(jnp.bfloat16)
    paired = jnp.concatenate([own_keys, own_values], axis=1)
    scale_factor = head_size ** (-0.5)

    def attend_block(running, key_block):
        block_keys = key_block[:, :head_size]
        block_values = key_block[:, head_size:]
        scores = (
            jnp.einsum("qd,kd->qk", query_rows, block_keys, preferred_element_type=jnp.float32)
            * scale_factor
        )
        weights = jnp.exp(scores)
        numer = running[0] + jnp.dot(
            weights.astype(jnp.bfloat16), block_values, preferred_element_type=jnp.float32
        )
        return (numer, running[1] + jnp.sum(weights, axis=1))

    zero_init = (
        jnp.zeros((local_heads * row_count, head_size), jnp.float32),
        jnp.zeros((local_heads * row_count,), jnp.float32),
    )
    running = zero_init
    gathered_piece = lax.all_gather(paired, "ep", axis=0, tiled=True)
    piece_rows = gathered_piece.shape[0]
    blocks = gathered_piece.reshape(piece_rows // 512, 512, gathered_piece.shape[1])

    def scan_block(partial_value, key_block):
        return (attend_block(partial_value, key_block), None)

    running, unused = lax.scan(scan_block, running, blocks)
    numer, denom = running
    head_out = (numer / denom[:, None]).astype(jnp.bfloat16)
    head_out = jnp.transpose(head_out.reshape(local_heads, row_count, head_size), (1, 0, 2))
    head_out = head_out.reshape(row_count, local_heads * head_size)
    mixed = lax.psum_scatter(
        jnp.dot(head_out, w_out, preferred_element_type=jnp.float32).astype(jnp.bfloat16),
        "tp",
        scatter_dimension=0,
        tiled=True,
    ).astype(jnp.float32)
    return head_norm(mixed, post_gain).astype(jnp.bfloat16)


def experts_half(moe_in, routes, route_logits, pre_gain, w_gate, w_up, w_down):
    token_count, top_count = routes.shape
    model_width = moe_in.shape[1]
    expert_count = lax.axis_size("ep")
    capacity = max(2, 3 * top_count * token_count // (2 * expert_count))
    tp_count = lax.axis_size("tp")
    slice_width = model_width // tp_count
    normed = head_norm(moe_in.astype(jnp.float32), pre_gain).astype(jnp.bfloat16)
    slot_owner, placed = slot_table(routes, expert_count, capacity)
    padded = jnp.concatenate([normed, jnp.zeros((1, model_width), jnp.bfloat16)], axis=0)
    outgoing = padded[slot_owner // top_count].reshape(expert_count, capacity, model_width)
    arrived = lax.all_to_all(outgoing, "ep", split_axis=0, concat_axis=0, tiled=True)
    arrived = arrived.reshape(expert_count * capacity, model_width)
    gate_pre = jnp.dot(arrived, w_gate[0], preferred_element_type=jnp.float32)
    up_pre = jnp.dot(arrived, w_up[0], preferred_element_type=jnp.float32)
    hidden = (jax.nn.silu(gate_pre) * up_pre).astype(jnp.bfloat16)
    partial_out = jnp.dot(hidden, w_down[0], preferred_element_type=jnp.float32)
    partial_out = partial_out.reshape(expert_count, capacity, model_width)
    summed = lax.psum_scatter(
        partial_out.astype(jnp.bfloat16), "tp", scatter_dimension=2, tiled=True
    )
    returned = lax.all_to_all(summed, "ep", split_axis=0, concat_axis=0, tiled=True)
    returned = returned.reshape(expert_count * capacity, slice_width)
    copies = returned[placed].reshape(token_count, top_count, slice_width).astype(jnp.float32)
    route_weight = jax.nn.softmax(route_logits, axis=-1)
    return jnp.sum(route_weight[..., None] * copies, axis=1).astype(jnp.bfloat16)


def per_device(
    q_in,
    k_in,
    v_in,
    q_gain,
    k_gain,
    w_out,
    post_gain,
    moe_in,
    routes,
    route_logits,
    pre_gain,
    w_gate,
    w_up,
    w_down,
):
    attn_out = mixer_half(q_in, k_in, v_in, q_gain, k_gain, w_out, post_gain)
    moe_out = experts_half(moe_in, routes, route_logits, pre_gain, w_gate, w_up, w_down)
    return (attn_out, moe_out)


def solution(mesh):
    return jax.shard_map(
        per_device,
        mesh=mesh,
        in_specs=(
            P("ep", "tp"),
            P("ep", None),
            P("ep", None),
            P(),
            P(),
            P("tp", None),
            P(),
            P("ep", None),
            P("ep", None),
            P("ep", None),
            P(),
            P("ep", None, "tp"),
            P("ep", None, "tp"),
            P("ep", "tp", None),
        ),
        out_specs=(P(("ep", "tp"), None), P("ep", "tp")),
        check_vma=False,
    )
```

profile of v0, /device:TPU:0, one launch (start us, length us, event | category | flops | bytes accessed | tf_op | source)
XLA Modules:
  0.0 186.0 jit_solution(11214696343545034479)
XLA Ops:
  11.1 1.4 scatter_custom_fusion
  12.5 1.2 fusion.22
  13.7 1.2 fusion.24
  15.0 3.1 %gather_fusion = bf16[384,2048]{1,0:T(8,128)(2,1)} fusion(bf16[129,2048]{1,0:T(8,128)(2,1)S(1)} %concatenate.17, s32[1024]{0:T(1024)S(1)} %pad_clamp_fusion.1), kind=kCustom, calls=%fused_computation | custom fusion | bytes 3147264 | tf_op jit(solution)/shard_map/gather | solution.py:129
  18.2 7.4 %all-to-all-start = ((bf16[8,48,2048]{2,1,0:T(8,128)(2,1)}), bf16[8,48,2048]{2,1,0:T(8,128)(2,1)}, u32[]{:S(2)}, u32[]{:S(2)}) async-start(bf16[8,48,2048]{2,1,0:T(8,128)(2,1)} %bitcast.13), calls=%async_computation.1 | async-start | bytes 3145728 | tf_op jit(solution)/shard_map/all_to_all | solution.py:130
  28.4 50.5 %all-gather.2.cloned.1.call-done = bf16[4096,128]{0,1:T(8,128)(2,1)} async-done(((bf16[512,128]{0,1:T(8,128)(2,1)}), bf16[4096,128]{0,1:T(8,128)(2,1)}) %all-gather.2.cloned.1.call-update) | async-done | bytes 1048592 | tf_op jit(solution)/shard_map/all_gather | solution.py:98
  78.9 1.6 copy.42
  80.6 4.6 %fusion.12 = f32[384,1024]{1,0:T(8,128)S(1)} fusion(bf16[384,2048]{1,0:T(8,128)(2,1)} %bitcast.14, bf16[1,2048,1024]{2,1,0:T(8,128)(2,1)} %param.27), kind=kOutput, calls=%fused_computation.18 | convolution fusion | flops 1610612736 | bytes 7340032 | tf_op jit(solution)/shard_map/dot_general | solution.py:132
  85.2 3.5 %multiply_convert_fusion = bf16[384,1024]{1,0:T(8,128)(2,1)S(1)} fusion(f32[384,1024]{1,0:T(8,128)S(1)} %fusion.12, bf16[384,2048]{1,0:T(8,128)(2,1)} %bitcast.14, bf16[1,2048,1024]{2,1,0:T(8,128)(2,1)S(1)} %copy-done.8), kind=kOutput, calls=%fused_computation.22 | convolution fusion | flops 1612972032 | bytes 8126464 | tf_op jit(solution)/shard_map/dot_general | solution.py:133
  88.8 3.0 %fusion.14 = bf16[8,48,2048]{2,1,0:T(8,128)(2,1)} fusion(bf16[8,48,1024]{2,1,0:T(8,128)(2,1)S(1)} %bitcast.62, bf16[1,1024,2048]{2,1,0:T(8,128)(2,1)S(1)} %copy-done.9), kind=kOutput, calls=%fused_computation.21 | convolution fusion | flops 1611399168 | bytes 6553600 | tf_op jit(solution)/shard_map/dot_general | solution.py:135
  91.8 46.4 %while.13 = (s32[]{:T(128)}, f32[2048,64]{0,1:T(8,128)S(1)}, f32[2048]{0:T(1024)S(1)}, bf16[8,512,128]{2,1,0:T(8,128)(2,1)S(1)}, bf16[2048,64]{1,0:T(8,128)(2,1)S(1)}, /*index=5*/s32[]{:T(128)}, s32[]{:T(128)}) while((s32[]{:T(128)}, f32[2048,64]{0,1:T(8,128)S(1)}, f32[2048]{0:T(1024)S(1)}, bf16[8,512,128]{2,1,0:T(8,128)(2,1)S(1)}, ...), condition=%wide.region_4.5_spmd.clone, body=%wide.region_2.4_spmd.clone.sunk | while | flops 272893952 | bytes 10256476 | solution.py:105
  91.9 2.7 %fusion.72 = (f32[2048]{0:T(1024)S(1)}, f32[512,2048]{1,0:T(8,128)}) fusion(bf16[2048,64]{1,0:T(8,128)(2,1)S(1)} %get-tuple-element.147, bf16[512,128]{1,0:T(8,128)(2,1)S(1)} %dynamic-slice_bitcast_fusion.2), kind=kOutput, calls=%fused_computation.4.clone.1 | convolution fusion | flops 136312832 | bytes 4595712 | tf_op jit(solution)/shard_map/while/body/eval_jaxpr/qd,kd->qk/dot_general | solution.py:84
  94.5 3.1 %convolution_add_fusion.2 = f32[2048,64]{0,1:T(8,128)S(1)} fusion(f32[512,2048]{1,0:T(8,128)} %get-tuple-element.127, f32[2048,64]{0,1:T(8,128)S(1)} %get-tuple-element.137, pred[]{:T(512)S(6)} %compare.19, bf16[512,128]{1,0:T(8,128)(2,1)S(1)} %dynamic-slice_bitcast_fusion.2), kind=kOutput, calls=%fused_computation.6.clone.1 | convolution fusion | flops 136577024 | bytes 5373953 | tf_op jit(solution)/shard_map/while/body/eval_jaxpr/dot_general | solution.py:88
  97.7 2.7 %fusion.72 = (f32[2048]{0:T(1024)S(1)}, f32[512,2048]{1,0:T(8,128)}) fusion(bf16[2048,64]{1,0:T(8,128)(2,1)S(1)} %get-tuple-element.147, bf16[512,128]{1,0:T(8,128)(2,1)S(1)} %dynamic-slice_bitcast_fusion.2), kind=kOutput, calls=%fused_computation.4.clone.1 | convolution fusion | flops 136312832 | bytes 4595712 | tf_op jit(solution)/shard_map/while/body/eval_jaxpr/qd,kd->qk/dot_general | solution.py:84
  100.3 3.2 %convolution_add_fusion.2 = f32[2048,64]{0,1:T(8,128)S(1)} fusion(f32[512,2048]{1,0:T(8,128)} %get-tuple-element.127, f32[2048,64]{0,1:T(8,128)S(1)} %get-tuple-element.137, pred[]{:T(512)S(6)} %compare.19, bf16[512,128]{1,0:T(8,128)(2,1)S(1)} %dynamic-slice_bitcast_fusion.2), kind=kOutput, calls=%fused_computation.6.clone.1 | convolution fusion | flops 136577024 | bytes 5373953 | tf_op jit(solution)/shard_map/while/body/eval_jaxpr/dot_general | solution.py:88
  103.5 2.7 %fusion.72 = (f32[2048]{0:T(1024)S(1)}, f32[512,2048]{1,0:T(8,128)}) fusion(bf16[2048,64]{1,0:T(8,128)(2,1)S(1)} %get-tuple-element.147, bf16[512,128]{1,0:T(8,128)(2,1)S(1)} %dynamic-slice_bitcast_fusion.2), kind=kOutput, calls=%fused_computation.4.clone.1 | convolution fusion | flops 136312832 | bytes 4595712 | tf_op jit(solution)/shard_map/while/body/eval_jaxpr/qd,kd->qk/dot_general | solution.py:84
  106.2 3.1 %convolution_add_fusion.2 = f32[2048,64]{0,1:T(8,128)S(1)} fusion(f32[512,2048]{1,0:T(8,128)} %get-tuple-element.127, f32[2048,64]{0,1:T(8,128)S(1)} %get-tuple-element.137, pred[]{:T(512)S(6)} %compare.19, bf16[512,128]{1,0:T(8,128)(2,1)S(1)} %dynamic-slice_bitcast_fusion.2), kind=kOutput, calls=%fused_computation.6.clone.1 | convolution fusion | flops 136577024 | bytes 5373953 | tf_op jit(solution)/shard_map/while/body/eval_jaxpr/dot_general | solution.py:88
  109.3 2.7 %fusion.72 = (f32[2048]{0:T(1024)S(1)}, f32[512,2048]{1,0:T(8,128)}) fusion(bf16[2048,64]{1,0:T(8,128)(2,1)S(1)} %get-tuple-element.147, bf16[512,128]{1,0:T(8,128)(2,1)S(1)} %dynamic-slice_bitcast_fusion.2), kind=kOutput, calls=%fused_computation.4.clone.1 | convolution fusion | flops 136312832 | bytes 4595712 | tf_op jit(solution)/shard_map/while/body/eval_jaxpr/qd,kd->qk/dot_general | solution.py:84
  112.0 3.1 %convolution_add_fusion.2 = f32[2048,64]{0,1:T(8,128)S(1)} fusion(f32[512,2048]{1,0:T(8,128)} %get-tuple-element.127, f32[2048,64]{0,1:T(8,128)S(1)} %get-tuple-element.137, pred[]{:T(512)S(6)} %compare.19, bf16[512,128]{1,0:T(8,128)(2,1)S(1)} %dynamic-slice_bitcast_fusion.2), kind=kOutput, calls=%fused_computation.6.clone.1 | convolution fusion | flops 136577024 | bytes 5373953 | tf_op jit(solution)/shard_map/while/body/eval_jaxpr/dot_general | solution.py:88
  115.1 2.7 %fusion.72 = (f32[2048]{0:T(1024)S(1)}, f32[512,2048]{1,0:T(8,128)}) fusion(bf16[2048,64]{1,0:T(8,128)(2,1)S(1)} %get-tuple-element.147, bf16[512,128]{1,0:T(8,128)(2,1)S(1)} %dynamic-slice_bitcast_fusion.2), kind=kOutput, calls=%fused_computation.4.clone.1 | convolution fusion | flops 136312832 | bytes 4595712 | tf_op jit(solution)/shard_map/while/body/eval_jaxpr/qd,kd->qk/dot_general | solution.py:84
  117.8 3.1 %convolution_add_fusion.2 = f32[2048,64]{0,1:T(8,128)S(1)} fusion(f32[512,2048]{1,0:T(8,128)} %get-tuple-element.127, f32[2048,64]{0,1:T(8,128)S(1)} %get-tuple-element.137, pred[]{:T(512)S(6)} %compare.19, bf16[512,128]{1,0:T(8,128)(2,1)S(1)} %dynamic-slice_bitcast_fusion.2), kind=kOutput, calls=%fused_computation.6.clone.1 | convolution fusion | flops 136577024 | bytes 5373953 | tf_op jit(solution)/shard_map/while/body/eval_jaxpr/dot_general | solution.py:88
  120.9 2.7 %fusion.72 = (f32[2048]{0:T(1024)S(1)}, f32[512,2048]{1,0:T(8,128)}) fusion(bf16[2048,64]{1,0:T(8,128)(2,1)S(1)} %get-tuple-element.147, bf16[512,128]{1,0:T(8,128)(2,1)S(1)} %dynamic-slice_bitcast_fusion.2), kind=kOutput, calls=%fused_computation.4.clone.1 | convolution fusion | flops 136312832 | bytes 4595712 | tf_op jit(solution)/shard_map/while/body/eval_jaxpr/qd,kd->qk/dot_general | solution.py:84
  123.6 3.1 %convolution_add_fusion.2 = f32[2048,64]{0,1:T(8,128)S(1)} fusion(f32[512,2048]{1,0:T(8,128)} %get-tuple-element.127, f32[2048,64]{0,1:T(8,128)S(1)} %get-tuple-element.137, pred[]{:T(512)S(6)} %compare.19, bf16[512,128]{1,0:T(8,128)(2,1)S(1)} %dynamic-slice_bitcast_fusion.2), kind=kOutput, calls=%fused_computation.6.clone.1 | convolution fusion | flops 136577024 | bytes 5373953 | tf_op jit(solution)/shard_map/while/body/eval_jaxpr/dot_general | solution.py:88
  126.7 2.7 %fusion.72 = (f32[2048]{0:T(1024)S(1)}, f32[512,2048]{1,0:T(8,128)}) fusion(bf16[2048,64]{1,0:T(8,128)(2,1)S(1)} %get-tuple-element.147, bf16[512,128]{1,0:T(8,128)(2,1)S(1)} %dynamic-slice_bitcast_fusion.2), kind=kOutput, calls=%fused_computation.4.clone.1 | convolution fusion | flops 136312832 | bytes 4595712 | tf_op jit(solution)/shard_map/while/body/eval_jaxpr/qd,kd->qk/dot_general | solution.py:84
  129.4 3.1 %convolution_add_fusion.2 = f32[2048,64]{0,1:T(8,128)S(1)} fusion(f32[512,2048]{1,0:T(8,128)} %get-tuple-element.127, f32[2048,64]{0,1:T(8,128)S(1)} %get-tuple-element.137, pred[]{:T(512)S(6)} %compare.19, bf16[512,128]{1,0:T(8,128)(2,1)S(1)} %dynamic-slice_bitcast_fusion.2), kind=kOutput, calls=%fused_computation.6.clone.1 | convolution fusion | flops 136577024 | bytes 5373953 | tf_op jit(solution)/shard_map/while/body/eval_jaxpr/dot_general | solution.py:88
  132.5 2.7 %fusion.72 = (f32[2048]{0:T(1024)S(1)}, f32[512,2048]{1,0:T(8,128)}) fusion(bf16[2048,64]{1,0:T(8,128)(2,1)S(1)} %get-tuple-element.147, bf16[512,128]{1,0:T(8,128)(2,1)S(1)} %dynamic-slice_bitcast_fusion.2), kind=kOutput, calls=%fused_computation.4.clone.1 | convolution fusion | flops 136312832 | bytes 4595712 | tf_op jit(solution)/shard_map/while/body/eval_jaxpr/qd,kd->qk/dot_general | solution.py:84
  135.2 3.1 %convolution_add_fusion.2 = f32[2048,64]{0,1:T(8,128)S(1)} fusion(f32[512,2048]{1,0:T(8,128)} %get-tuple-element.127, f32[2048,64]{0,1:T(8,128)S(1)} %get-tuple-element.137, pred[]{:T(512)S(6)} %compare.19, bf16[512,128]{1,0:T(8,128)(2,1)S(1)} %dynamic-slice_bitcast_fusion.2), kind=kOutput, calls=%fused_computation.6.clone.1 | convolution fusion | flops 136577024 | bytes 5373953 | tf_op jit(solution)/shard_map/while/body/eval_jaxpr/dot_general | solution.py:88
  138.6 2.1 %convolution_convert_fusion = bf16[512,2048]{1,0:T(8,128)(2,1)} fusion(bf16[512,256]{0,1:T(8,128)(2,1)S(1)} %bitcast.57, bf16[256,2048]{1,0:T(8,128)(2,1)S(1)} %copy-done), kind=kOutput, calls=%fused_computation.20 | convolution fusion | flops 537919488 | bytes 3407872 | tf_op jit(solution)/shard_map/dot_general | solution.py:111
  141.6 5.0 %all-to-all-start.1 = ((bf16[8,48,512]{2,1,0:T(8,128)(2,1)}), bf16[8,48,512]{2,1,0:T(8,128)(2,1)S(1)}, u32[]{:S(2)}, u32[]{:S(2)}) async-start(bf16[8,48,512]{2,1,0:T(8,128)(2,1)} %reduce-scatter.5.cloned.1.call-done), calls=%async_computation.3 | async-start | bytes 786432 | tf_op jit(solution)/shard_map/all_to_all | solution.py:140
  146.6 25.8 %reduce-scatter.3.cloned.1.call-done = bf16[128,2048]{1,0:T(8,128)(2,1)} async-done(((bf16[512,2048]{1,0:T(8,128)(2,1)}), bf16[128,2048]{1,0:T(8,128)(2,1)}) %reduce-scatter.3.cloned.1.call-update) | async-done | bytes 524304 | tf_op jit(solution)/shard_map/reduce_scatter | solution.py:110
  173.7 2.0 %fusion.21 = bf16[128,2048]{1,0:T(8,128)(2,1)} fusion(bf16[128,2048]{1,0:T(8,128)(2,1)} %reduce-scatter.3.cloned.1.call-done, f32[2048]{0:T(1024)S(1)} %copy-done.5, f32[128]{0:T(128)S(1)} %add_rsqrt_fusion.3), kind=kLoop, calls=%fused_computation.29 | loop fusion | flops 1048576 | bytes 1057280 | tf_op jit(solution)/shard_map/convert_element_type | solution.py:116
  177.2 1.4 multiply_reduce_fusion
  (96 shorter events, 9.8 us)
Async XLA Ops:
  8.0 130.6 %copy-start = (bf16[256,2048]{1,0:T(8,128)(2,1)S(1)}, bf16[256,2048]{1,0:T(8,128)(2,1)}, u32[]{:S(2)}) copy-start(bf16[256,2048]{1,0:T(8,128)(2,1)} %param.21) | copy-start | bytes 3145732
  18.1 7.5 %copy-start.2 = (bf16[512,256]{1,0:T(8,128)(2,1)S(1)}, bf16[512,256]{1,0:T(8,128)(2,1)}, u32[]{:S(2)}) copy-start(bf16[512,256]{1,0:T(8,128)(2,1)} %param.18) | copy-start | bytes 786436
  18.2 7.5 %copy-start.3 = (bf16[512,256]{1,0:T(8,128)(2,1)S(1)}, bf16[512,256]{1,0:T(8,128)(2,1)}, u32[]{:S(2)}) copy-start(bf16[512,256]{1,0:T(8,128)(2,1)} %param.17) | copy-start | bytes 786436
  18.2 8.0 %copy-start.6 = (f32[64]{0:T(128)S(1)}, f32[64]{0:T(128)}, u32[]{:S(2)}) copy-start(f32[64]{0:T(128)} %param.20) | copy-start | bytes 772
  18.2 9.2 %copy-start.1 = (bf16[512,256]{1,0:T(8,128)(2,1)S(1)}, bf16[512,256]{1,0:T(8,128)(2,1)}, u32[]{:S(2)}) copy-start(bf16[512,256]{1,0:T(8,128)(2,1)} %param.16) | copy-start | bytes 786436
  18.2 62.4 %all-to-all-start = ((bf16[8,48,2048]{2,1,0:T(8,128)(2,1)}), bf16[8,48,2048]{2,1,0:T(8,128)(2,1)}, u32[]{:S(2)}, u32[]{:S(2)}) async-start(bf16[8,48,2048]{2,1,0:T(8,128)(2,1)} %bitcast.13), calls=%async_computation.1 | async-start | bytes 3145728 | tf_op jit(solution)/shard_map/all_to_all | solution.py:130
  25.6 2.3 %copy-start.7 = (f32[64]{0:T(128)S(1)}, f32[64]{0:T(128)}, u32[]{:S(2)}) copy-start(f32[64]{0:T(128)} %param.19) | copy-start | bytes 772
  25.6 53.3 %all-gather.2.cloned.1.call-start = ((), (), s32[]{:S(2)}) async-start(), calls=%async_computation.4 | async-start | bytes 1179648 | tf_op jit(solution)/shard_map/all_gather | solution.py:98
  27.2 114.3 %reduce-scatter.5.cloned.1.call-start = ((), (), s32[]{:S(2)}) async-start(), calls=%async_computation.6 | async-start | bytes 1966080 | tf_op jit(solution)/shard_map/reduce_scatter | solution.py:137
  80.6 4.6 %copy-start.8 = (bf16[1,2048,1024]{2,1,0:T(8,128)(2,1)S(1)}, bf16[1,2048,1024]{2,1,0:T(8,128)(2,1)}, u32[]{:S(2)}) copy-start(bf16[1,2048,1024]{2,1,0:T(8,128)(2,1)} %param.28) | copy-start | bytes 12582916
  85.2 3.6 %copy-start.9 = (bf16[1,1024,2048]{2,1,0:T(8,128)(2,1)S(1)}, bf16[1,1024,2048]{2,1,0:T(8,128)(2,1)}, u32[]{:S(2)}) copy-start(bf16[1,1024,2048]{2,1,0:T(8,128)(2,1)} %param.29) | copy-start | bytes 12582916
  91.8 80.6 %reduce-scatter.3.cloned.1.call-start = ((), (), s32[]{:S(2)}) async-start(), calls=%async_computation.5 | async-start | bytes 2621440 | tf_op jit(solution)/shard_map/reduce_scatter | solution.py:110
  140.7 0.7 copy-start.4
  140.7 33.0 %copy-start.5 = (f32[2048]{0:T(1024)S(1)}, f32[2048]{0:T(1024)}, u32[]{:S(2)}) copy-start(f32[2048]{0:T(1024)} %param.22) | copy-start | bytes 24580
  141.6 34.1 %all-to-all-start.1 = ((bf16[8,48,512]{2,1,0:T(8,128)(2,1)}), bf16[8,48,512]{2,1,0:T(8,128)(2,1)S(1)}, u32[]{:S(2)}, u32[]{:S(2)}) async-start(bf16[8,48,512]{2,1,0:T(8,128)(2,1)} %reduce-scatter.5.cloned.1.call-done), calls=%async_computation.3 | async-start | bytes 786432 | tf_op jit(solution)/shard_map/all_to_all | solution.py:140
Sparse Core Ops, SparseCore 0:
  29.0 49.8 all-gather.1
Sparse Core Ops, SparseCore 1:
  91.9 28.3 reduce-scatter.4
  140.8 31.6 reduce-scatter.2
where the time goes:
time: 187 us; the launch traced here: 186 us
  waiting for transfers between devices  76.5 us (41%)
  matrix products  59.2 us (32%)
  between operations  15.9 us (9%)
  starting transfers between devices  12.5 us (7%)
  local copies, waits for them, and re-layouts  11.2 us (6%)
  other arithmetic  10.4 us (6%)
    all_gather x1, waiting for transfers between devices, mixer_half(): gathered_piece = lax.all_gather(paired, 'ep', axis=0, tiled=True)  50.5 us
    reduce_scatter x1, waiting for transfers between devices, mixer_half(): lax.psum_scatter(jnp.dot(head_out, w_out, preferred_element_type=jnp.floa...  25.8 us
    dot_general x8, matrix products, attend_block(): jnp.dot(weights.astype(jnp.bfloat16), block_values, preferred_element_typ...  24.7 us
    dot_general x8, matrix products, attend_block(): jnp.einsum('qd,kd->qk', query_rows, block_keys, preferred_element_type=jn...  21.2 us
    all_to_all x1, starting transfers between devices, experts_half(): lax.all_to_all(outgoing, 'ep', split_axis=0, concat_axis=0, tiled=True)  7.42 us
    all_to_all x1, starting transfers between devices, experts_half(): lax.all_to_all(summed, 'ep', split_axis=0, concat_axis=0, tiled=True)  4.98 us
    dot_general x1, matrix products, experts_half(): gate_pre = jnp.dot(arrived, w_gate[0], preferred_element_type=jnp.float32)  4.59 us
    unnamed x26, local copies, waits for them, and re-layouts  3.79 us
  transfers between devices with their start and end apart: 5, of which 2 were waited for; matrix products, arithmetic and copies ran while one was open for 30% of the time, Pallas kernels for 0%

commit v1 on v0

--- a/solution.py
+++ b/solution.py
@@ -6,6 +6,18 @@
 GRID_W = 128
 EPSILON = 1e-06
 ROPE_BASE = 10000.0
+
+
+def collect(x, axis, dim):
+    ways, here = (lax.axis_size(axis), lax.axis_index(axis))
+    grown, reach = (x, 1)
+    while reach < ways:
+        theirs = lax.ppermute(grown, axis, [(d, d ^ reach) for d in range(ways)])
+        mine_first = jnp.concatenate([grown, theirs], axis=dim)
+        theirs_first = jnp.concatenate([theirs, grown], axis=dim)
+        grown = jnp.where(here & reach == 0, mine_first, theirs_first)
+        reach = 2 * reach
+    return grown
 
 
 def head_norm(values, gain):
@@ -95,7 +107,7 @@
         jnp.zeros((local_heads * row_count,), jnp.float32),
     )
     running = zero_init
-    gathered_piece = lax.all_gather(paired, "ep", axis=0, tiled=True)
+    gathered_piece = collect(paired, "ep", 0)
     piece_rows = gathered_piece.shape[0]
     blocks = gathered_piece.reshape(piece_rows // 512, 512, gathered_piece.shape[1])
 

time: 187 us -> 233 us (1.25)
  waiting for transfers between devices: 76.5 us -> 109 us
  starting transfers between devices: 12.5 us -> 20.1 us
  local copies, waits for them, and re-layouts: 11.2 us -> 18.5 us
    ppermute x0 -> x3, waiting for transfers between devices: none -> 51.6 us  [collect(): theirs = lax.ppermute(grown, axis, [(d, d ^ reach) for d in range(ways)])]
    all_gather x1 -> x0, waiting for transfers between devices: 50.5 us -> none  [mixer_half(): gathered_piece = lax.all_gather(paired, 'ep', axis=0, tiled=True)]
    reduce_scatter x1, waiting for transfers between devices: 0.03 us -> 29.3 us  [experts_half(): lax.psum_scatter(partial_out.astype(jnp.bfloat16), 'tp', scatter_dimensio...]
    all_to_all x1, waiting for transfers between devices: 0.01 us -> 9.53 us  [experts_half(): lax.all_to_all(summed, 'ep', split_axis=0, concat_axis=0, tiled=True)]
    ppermute x0 -> x3, starting transfers between devices: none -> 9.35 us  [collect(): theirs = lax.ppermute(grown, axis, [(d, d ^ reach) for d in range(ways)])]
    reduce_scatter x1, waiting for transfers between devices: 25.8 us -> 18.6 us  [mixer_half(): lax.psum_scatter(jnp.dot(head_out, w_out, preferred_element_type=jnp.floa...]
    squeeze x8, local copies, waits for them, and re-layouts: 0.12 us -> 7.33 us  [mixer_half(): running, unused = lax.scan(scan_block, running, blocks)]
    all_to_all x1, starting transfers between devices: 7.42 us -> 5.01 us  [experts_half(): lax.all_to_all(outgoing, 'ep', split_axis=0, concat_axis=0, tiled=True)]
  transfers between devices with their start and end apart: 5 -> 7, of which waited for: 2 -> 5; matrix products, arithmetic and copies ran while one was open for 30% -> 36% of each run, Pallas kernels for 0% -> 0%
where the time goes in v1:
time: 233 us; the launch traced here: 232 us
  waiting for transfers between devices  109 us (47%)
  matrix products  59.1 us (25%)
  starting transfers between devices  20.1 us (9%)
  local copies, waits for them, and re-layouts  18.5 us (8%)
  between operations  14.5 us (6%)
  other arithmetic  10.3 us (4%)
    ppermute x3, waiting for transfers between devices, collect(): theirs = lax.ppermute(grown, axis, [(d, d ^ reach) for d in range(ways)])  51.6 us
    reduce_scatter x1, waiting for transfers between devices, experts_half(): lax.psum_scatter(partial_out.astype(jnp.bfloat16), 'tp', scatter_dimensio...  29.3 us
    dot_general x8, matrix products, attend_block(): jnp.dot(weights.astype(jnp.bfloat16), block_values, preferred_element_typ...  24.6 us
    dot_general x8, matrix products, attend_block(): jnp.einsum('qd,kd->qk', query_rows, block_keys, preferred_element_type=jn...  21.2 us
    reduce_scatter x1, waiting for transfers between devices, mixer_half(): lax.psum_scatter(jnp.dot(head_out, w_out, preferred_element_type=jnp.floa...  18.6 us
    all_to_all x1, waiting for transfers between devices, experts_half(): lax.all_to_all(summed, 'ep', split_axis=0, concat_axis=0, tiled=True)  9.53 us
    ppermute x3, starting transfers between devices, collect(): theirs = lax.ppermute(grown, axis, [(d, d ^ reach) for d in range(ways)])  9.35 us
    squeeze x8, local copies, waits for them, and re-layouts, mixer_half(): running, unused = lax.scan(scan_block, running, blocks)  7.33 us
  transfers between devices with their start and end apart: 7, of which 5 were waited for; matrix products, arithmetic and copies ran while one was open for 36% of the time, Pallas kernels for 0%

profile of v1, /device:TPU:0, one launch (start us, length us, event | category | flops | bytes accessed | tf_op | source)
XLA Modules:
  0.0 231.9 jit_solution(6665707826251025108)
XLA Ops:
  9.8 3.0 %collective-permute-start = (bf16[512,128]{0,1:T(8,128)(2,1)S(1)}, bf16[512,128]{0,1:T(8,128)(2,1)S(1)}, u32[]{:S(2)}, u32[]{:S(2)}) collective-permute-start(bf16[512,128]{0,1:T(8,128)(2,1)S(1)} %pad_maximum_fusion), channel_id=1, source_target_pairs={{0,4},{4,0},{8,12},{12,8},{16,20},{20,16},{24,28},{28,24},{1,5},{5... | collective-permute-start | bytes 393224 | tf_op jit(solution)/shard_map/ppermute | solution.py:15
  17.7 3.1 %gather_fusion = bf16[384,2048]{1,0:T(8,128)(2,1)} fusion(bf16[129,2048]{1,0:T(8,128)(2,1)S(1)} %concatenate.41, s32[1024]{0:T(1024)S(1)} %pad_clamp_fusion.1), kind=kCustom, calls=%fused_computation | custom fusion | bytes 3147264 | tf_op jit(solution)/shard_map/gather | solution.py:141
  20.9 5.0 %all-to-all-start = ((bf16[8,48,2048]{2,1,0:T(8,128)(2,1)}), bf16[8,48,2048]{2,1,0:T(8,128)(2,1)}, u32[]{:S(2)}, u32[]{:S(2)}) async-start(bf16[8,48,2048]{2,1,0:T(8,128)(2,1)} %bitcast.13), calls=%async_computation.1 | async-start | bytes 3145728 | tf_op jit(solution)/shard_map/all_to_all | solution.py:142
  26.3 2.0 collective-permute-start.1
  28.5 28.7 %collective-permute-done.1 = bf16[1024,128]{0,1:T(8,128)(2,1)S(1)} collective-permute-done((bf16[1024,128]{0,1:T(8,128)(2,1)S(1)}, bf16[1024,128]{0,1:T(8,128)(2,1)S(1)}, u32[]{:S(2)}, u32[]{:S(2)}) %collective-permute-start.1) | collective-permute-done | bytes 262176 | tf_op jit(solution)/shard_map/ppermute | solution.py:15
  57.3 4.3 %collective-permute-start.2 = (bf16[2048,128]{0,1:T(8,128)(2,1)S(1)}, bf16[2048,128]{0,1:T(8,128)(2,1)}, u32[]{:S(2)}, u32[]{:S(2)}) collective-permute-start(bf16[2048,128]{0,1:T(8,128)(2,1)S(1)} %maximum_select_fusion.1), channel_id=1, source_target_pairs={{0,16},{4,20},{8,24},{12,28},{16,0},{20,4},{24,8},{28,12},{1,17},{... | collective-permute-start | bytes 1572872 | tf_op jit(solution)/shard_map/ppermute | solution.py:15
  62.3 22.9 %collective-permute-done.2 = bf16[2048,128]{0,1:T(8,128)(2,1)} collective-permute-done((bf16[2048,128]{0,1:T(8,128)(2,1)S(1)}, bf16[2048,128]{0,1:T(8,128)(2,1)}, u32[]{:S(2)}, u32[]{:S(2)}) %collective-permute-start.2) | collective-permute-done | bytes 524320 | tf_op jit(solution)/shard_map/ppermute | solution.py:15
  88.3 53.4 %while.13 = (s32[]{:T(128)}, f32[2048,64]{0,1:T(8,128)S(1)}, f32[2048]{0:T(1024)S(1)}, bf16[8,512,128]{2,1,0:T(8,128)(2,1)}, bf16[2048,64]{1,0:T(8,128)(2,1)S(1)}, /*index=5*/s32[]{:T(128)}, s32[]{:T(128)}) while((s32[]{:T(128)}, f32[2048,64]{0,1:T(8,128)S(1)}, f32[2048]{0:T(1024)S(1)}, bf16[8,512,128]{2,1,0:T(8,128)(2,1)}, ...), condition=%wide.region_4.5_spmd.clone, body=%wide.region_2.4_spmd.clone.sunk | while | flops 272893952 | bytes 10256476 | solution.py:117
  89.2 2.7 %fusion.72 = (f32[2048]{0:T(1024)S(1)}, f32[512,2048]{1,0:T(8,128)}) fusion(bf16[2048,64]{1,0:T(8,128)(2,1)S(1)} %get-tuple-element.147, bf16[512,128]{1,0:T(8,128)(2,1)S(1)} %dynamic-slice_bitcast_fusion.2), kind=kOutput, calls=%fused_computation.4.clone.1 | convolution fusion | flops 136312832 | bytes 4595712 | tf_op jit(solution)/shard_map/while/body/eval_jaxpr/qd,kd->qk/dot_general | solution.py:96
  91.9 3.1 %convolution_add_fusion.2 = f32[2048,64]{0,1:T(8,128)S(1)} fusion(f32[512,2048]{1,0:T(8,128)} %get-tuple-element.127, f32[2048,64]{0,1:T(8,128)S(1)} %get-tuple-element.137, pred[]{:T(512)S(6)} %compare.19, bf16[512,128]{1,0:T(8,128)(2,1)S(1)} %dynamic-slice_bitcast_fusion.2), kind=kOutput, calls=%fused_computation.6.clone.1 | convolution fusion | flops 136577024 | bytes 5373953 | tf_op jit(solution)/shard_map/while/body/eval_jaxpr/dot_general | solution.py:100
  95.9 2.7 %fusion.72 = (f32[2048]{0:T(1024)S(1)}, f32[512,2048]{1,0:T(8,128)}) fusion(bf16[2048,64]{1,0:T(8,128)(2,1)S(1)} %get-tuple-element.147, bf16[512,128]{1,0:T(8,128)(2,1)S(1)} %dynamic-slice_bitcast_fusion.2), kind=kOutput, calls=%fused_computation.4.clone.1 | convolution fusion | flops 136312832 | bytes 4595712 | tf_op jit(solution)/shard_map/while/body/eval_jaxpr/qd,kd->qk/dot_general | solution.py:96
  98.6 3.1 %convolution_add_fusion.2 = f32[2048,64]{0,1:T(8,128)S(1)} fusion(f32[512,2048]{1,0:T(8,128)} %get-tuple-element.127, f32[2048,64]{0,1:T(8,128)S(1)} %get-tuple-element.137, pred[]{:T(512)S(6)} %compare.19, bf16[512,128]{1,0:T(8,128)(2,1)S(1)} %dynamic-slice_bitcast_fusion.2), kind=kOutput, calls=%fused_computation.6.clone.1 | convolution fusion | flops 136577024 | bytes 5373953 | tf_op jit(solution)/shard_map/while/body/eval_jaxpr/dot_general | solution.py:100
  102.6 2.7 %fusion.72 = (f32[2048]{0:T(1024)S(1)}, f32[512,2048]{1,0:T(8,128)}) fusion(bf16[2048,64]{1,0:T(8,128)(2,1)S(1)} %get-tuple-element.147, bf16[512,128]{1,0:T(8,128)(2,1)S(1)} %dynamic-slice_bitcast_fusion.2), kind=kOutput, calls=%fused_computation.4.clone.1 | convolution fusion | flops 136312832 | bytes 4595712 | tf_op jit(solution)/shard_map/while/body/eval_jaxpr/qd,kd->qk/dot_general | solution.py:96
  105.2 3.1 %convolution_add_fusion.2 = f32[2048,64]{0,1:T(8,128)S(1)} fusion(f32[512,2048]{1,0:T(8,128)} %get-tuple-element.127, f32[2048,64]{0,1:T(8,128)S(1)} %get-tuple-element.137, pred[]{:T(512)S(6)} %compare.19, bf16[512,128]{1,0:T(8,128)(2,1)S(1)} %dynamic-slice_bitcast_fusion.2), kind=kOutput, calls=%fused_computation.6.clone.1 | convolution fusion | flops 136577024 | bytes 5373953 | tf_op jit(solution)/shard_map/while/body/eval_jaxpr/dot_general | solution.py:100
  109.3 2.7 %fusion.72 = (f32[2048]{0:T(1024)S(1)}, f32[512,2048]{1,0:T(8,128)}) fusion(bf16[2048,64]{1,0:T(8,128)(2,1)S(1)} %get-tuple-element.147, bf16[512,128]{1,0:T(8,128)(2,1)S(1)} %dynamic-slice_bitcast_fusion.2), kind=kOutput, calls=%fused_computation.4.clone.1 | convolution fusion | flops 136312832 | bytes 4595712 | tf_op jit(solution)/shard_map/while/body/eval_jaxpr/qd,kd->qk/dot_general | solution.py:96
  111.9 3.1 %convolution_add_fusion.2 = f32[2048,64]{0,1:T(8,128)S(1)} fusion(f32[512,2048]{1,0:T(8,128)} %get-tuple-element.127, f32[2048,64]{0,1:T(8,128)S(1)} %get-tuple-element.137, pred[]{:T(512)S(6)} %compare.19, bf16[512,128]{1,0:T(8,128)(2,1)S(1)} %dynamic-slice_bitcast_fusion.2), kind=kOutput, calls=%fused_computation.6.clone.1 | convolution fusion | flops 136577024 | bytes 5373953 | tf_op jit(solution)/shard_map/while/body/eval_jaxpr/dot_general | solution.py:100
  115.9 2.7 %fusion.72 = (f32[2048]{0:T(1024)S(1)}, f32[512,2048]{1,0:T(8,128)}) fusion(bf16[2048,64]{1,0:T(8,128)(2,1)S(1)} %get-tuple-element.147, bf16[512,128]{1,0:T(8,128)(2,1)S(1)} %dynamic-slice_bitcast_fusion.2), kind=kOutput, calls=%fused_computation.4.clone.1 | convolution fusion | flops 136312832 | bytes 4595712 | tf_op jit(solution)/shard_map/while/body/eval_jaxpr/qd,kd->qk/dot_general | solution.py:96
  118.6 3.1 %convolution_add_fusion.2 = f32[2048,64]{0,1:T(8,128)S(1)} fusion(f32[512,2048]{1,0:T(8,128)} %get-tuple-element.127, f32[2048,64]{0,1:T(8,128)S(1)} %get-tuple-element.137, pred[]{:T(512)S(6)} %compare.19, bf16[512,128]{1,0:T(8,128)(2,1)S(1)} %dynamic-slice_bitcast_fusion.2), kind=kOutput, calls=%fused_computation.6.clone.1 | convolution fusion | flops 136577024 | bytes 5373953 | tf_op jit(solution)/shard_map/while/body/eval_jaxpr/dot_general | solution.py:100
  122.6 2.7 %fusion.72 = (f32[2048]{0:T(1024)S(1)}, f32[512,2048]{1,0:T(8,128)}) fusion(bf16[2048,64]{1,0:T(8,128)(2,1)S(1)} %get-tuple-element.147, bf16[512,128]{1,0:T(8,128)(2,1)S(1)} %dynamic-slice_bitcast_fusion.2), kind=kOutput, calls=%fused_computation.4.clone.1 | convolution fusion | flops 136312832 | bytes 4595712 | tf_op jit(solution)/shard_map/while/body/eval_jaxpr/qd,kd->qk/dot_general | solution.py:96
  125.3 3.1 %convolution_add_fusion.2 = f32[2048,64]{0,1:T(8,128)S(1)} fusion(f32[512,2048]{1,0:T(8,128)} %get-tuple-element.127, f32[2048,64]{0,1:T(8,128)S(1)} %get-tuple-element.137, pred[]{:T(512)S(6)} %compare.19, bf16[512,128]{1,0:T(8,128)(2,1)S(1)} %dynamic-slice_bitcast_fusion.2), kind=kOutput, calls=%fused_computation.6.clone.1 | convolution fusion | flops 136577024 | bytes 5373953 | tf_op jit(solution)/shard_map/while/body/eval_jaxpr/dot_general | solution.py:100
  129.3 2.7 %fusion.72 = (f32[2048]{0:T(1024)S(1)}, f32[512,2048]{1,0:T(8,128)}) fusion(bf16[2048,64]{1,0:T(8,128)(2,1)S(1)} %get-tuple-element.147, bf16[512,128]{1,0:T(8,128)(2,1)S(1)} %dynamic-slice_bitcast_fusion.2), kind=kOutput, calls=%fused_computation.4.clone.1 | convolution fusion | flops 136312832 | bytes 4595712 | tf_op jit(solution)/shard_map/while/body/eval_jaxpr/qd,kd->qk/dot_general | solution.py:96
  132.0 3.1 %convolution_add_fusion.2 = f32[2048,64]{0,1:T(8,128)S(1)} fusion(f32[512,2048]{1,0:T(8,128)} %get-tuple-element.127, f32[2048,64]{0,1:T(8,128)S(1)} %get-tuple-element.137, pred[]{:T(512)S(6)} %compare.19, bf16[512,128]{1,0:T(8,128)(2,1)S(1)} %dynamic-slice_bitcast_fusion.2), kind=kOutput, calls=%fused_computation.6.clone.1 | convolution fusion | flops 136577024 | bytes 5373953 | tf_op jit(solution)/shard_map/while/body/eval_jaxpr/dot_general | solution.py:100
  136.0 2.7 %fusion.72 = (f32[2048]{0:T(1024)S(1)}, f32[512,2048]{1,0:T(8,128)}) fusion(bf16[2048,64]{1,0:T(8,128)(2,1)S(1)} %get-tuple-element.147, bf16[512,128]{1,0:T(8,128)(2,1)S(1)} %dynamic-slice_bitcast_fusion.2), kind=kOutput, calls=%fused_computation.4.clone.1 | convolution fusion | flops 136312832 | bytes 4595712 | tf_op jit(solution)/shard_map/while/body/eval_jaxpr/qd,kd->qk/dot_general | solution.py:96
  138.6 3.1 %convolution_add_fusion.2 = f32[2048,64]{0,1:T(8,128)S(1)} fusion(f32[512,2048]{1,0:T(8,128)} %get-tuple-element.127, f32[2048,64]{0,1:T(8,128)S(1)} %get-tuple-element.137, pred[]{:T(512)S(6)} %compare.19, bf16[512,128]{1,0:T(8,128)(2,1)S(1)} %dynamic-slice_bitcast_fusion.2), kind=kOutput, calls=%fused_computation.6.clone.1 | convolution fusion | flops 136577024 | bytes 5373953 | tf_op jit(solution)/shard_map/while/body/eval_jaxpr/dot_general | solution.py:100
  142.1 2.1 convolution_convert_fusion
  144.4 4.6 %fusion.12 = f32[384,1024]{1,0:T(8,128)S(1)} fusion(bf16[384,2048]{1,0:T(8,128)(2,1)} %bitcast.14, bf16[1,2048,1024]{2,1,0:T(8,128)(2,1)} %param.27), kind=kOutput, calls=%fused_computation.18 | convolution fusion | flops 1610612736 | bytes 7340032 | tf_op jit(solution)/shard_map/dot_general | solution.py:144
  149.1 3.6 %multiply_convert_fusion = bf16[384,1024]{1,0:T(8,128)(2,1)S(1)} fusion(f32[384,1024]{1,0:T(8,128)S(1)} %fusion.12, bf16[384,2048]{1,0:T(8,128)(2,1)} %bitcast.14, bf16[1,2048,1024]{2,1,0:T(8,128)(2,1)S(1)} %copy-done.8), kind=kOutput, calls=%fused_computation.22 | convolution fusion | flops 1612972032 | bytes 8126464 | tf_op jit(solution)/shard_map/dot_general | solution.py:145
  152.7 3.0 %fusion.14 = bf16[8,48,2048]{2,1,0:T(8,128)(2,1)} fusion(bf16[8,48,1024]{2,1,0:T(8,128)(2,1)S(1)} %bitcast.62, bf16[1,1024,2048]{2,1,0:T(8,128)(2,1)S(1)} %copy-done.9), kind=kOutput, calls=%fused_computation.21 | convolution fusion | flops 1611399168 | bytes 6553600 | tf_op jit(solution)/shard_map/dot_general | solution.py:147
  155.9 18.6 %reduce-scatter.3.cloned.1.call-done = bf16[128,2048]{1,0:T(8,128)(2,1)} async-done(((bf16[512,2048]{1,0:T(8,128)(2,1)}), bf16[128,2048]{1,0:T(8,128)(2,1)}) %reduce-scatter.3.cloned.1.call-update) | async-done | bytes 524304 | tf_op jit(solution)/shard_map/reduce_scatter | solution.py:122
  175.8 29.3 %reduce-scatter.5.cloned.1.call-done = bf16[8,48,512]{2,1,0:T(8,128)(2,1)} async-done(((bf16[8,48,2048]{2,1,0:T(8,128)(2,1)}), bf16[8,48,512]{2,1,0:T(8,128)(2,1)}) %reduce-scatter.5.cloned.1.call-update) | async-done | bytes 393232 | tf_op jit(solution)/shard_map/reduce_scatter | solution.py:149
  205.1 5.5 %all-to-all-start.1 = ((bf16[8,48,512]{2,1,0:T(8,128)(2,1)}), bf16[8,48,512]{2,1,0:T(8,128)(2,1)S(1)}, u32[]{:S(2)}, u32[]{:S(2)}) async-start(bf16[8,48,512]{2,1,0:T(8,128)(2,1)} %reduce-scatter.5.cloned.1.call-done), calls=%async_computation.3 | async-start | bytes 786432 | tf_op jit(solution)/shard_map/all_to_all | solution.py:152
  212.7 9.5 %all-to-all-done.1 = bf16[8,48,512]{2,1,0:T(8,128)(2,1)S(1)} async-done(((bf16[8,48,512]{2,1,0:T(8,128)(2,1)}), bf16[8,48,512]{2,1,0:T(8,128)(2,1)S(1)}, u32[]{:S(2)}, u32[]{:S(2)}) %all-to-all-start.1) | async-done | bytes 393248 | tf_op jit(solution)/shard_map/all_to_all | solution.py:152
  (102 shorter events, 26.0 us)
Async XLA Ops:
  7.2 134.9 %copy-start = (bf16[256,2048]{1,0:T(8,128)(2,1)S(1)}, bf16[256,2048]{1,0:T(8,128)(2,1)}, u32[]{:S(2)}) copy-start(bf16[256,2048]{1,0:T(8,128)(2,1)} %param.21) | copy-start | bytes 3145732
  7.2 10.1 %copy-start.2 = (bf16[128,2048]{1,0:T(8,128)(2,1)S(1)}, bf16[128,2048]{1,0:T(8,128)(2,1)}, u32[]{:S(2)}) copy-start(bf16[128,2048]{1,0:T(8,128)(2,1)} %param.23) | copy-start | bytes 1572868
  7.2 10.3 %copy-start.5 = (f32[2048]{0:T(1024)S(1)}, f32[2048]{0:T(1024)}, u32[]{:S(2)}) copy-start(f32[2048]{0:T(1024)} %param.26) | copy-start | bytes 24580
  9.8 16.3 %collective-permute-start = (bf16[512,128]{0,1:T(8,128)(2,1)S(1)}, bf16[512,128]{0,1:T(8,128)(2,1)S(1)}, u32[]{:S(2)}, u32[]{:S(2)}) collective-permute-start(bf16[512,128]{0,1:T(8,128)(2,1)S(1)} %pad_maximum_fusion), channel_id=1, source_target_pairs={{0,4},{4,0},{8,12},{12,8},{16,20},{20,16},{24,28},{28,24},{1,5},{5... | collective-permute-start | bytes 393224 | tf_op jit(solution)/shard_map/ppermute | solution.py:15
  20.9 5.1 %copy-start.3 = (bf16[512,256]{1,0:T(8,128)(2,1)S(1)}, bf16[512,256]{1,0:T(8,128)(2,1)}, u32[]{:S(2)}) copy-start(bf16[512,256]{1,0:T(8,128)(2,1)} %param.16) | copy-start | bytes 786436
  20.9 7.5 %copy-start.7 = (f32[64]{0:T(128)S(1)}, f32[64]{0:T(128)}, u32[]{:S(2)}) copy-start(f32[64]{0:T(128)} %param.19) | copy-start | bytes 772
  20.9 123.5 %all-to-all-start = ((bf16[8,48,2048]{2,1,0:T(8,128)(2,1)}), bf16[8,48,2048]{2,1,0:T(8,128)(2,1)}, u32[]{:S(2)}, u32[]{:S(2)}) async-start(bf16[8,48,2048]{2,1,0:T(8,128)(2,1)} %bitcast.13), calls=%async_computation.1 | async-start | bytes 3145728 | tf_op jit(solution)/shard_map/all_to_all | solution.py:142
  25.9 148.7 %reduce-scatter.3.cloned.1.call-start = ((), (), s32[]{:S(2)}) async-start(), calls=%async_computation.4 | async-start | bytes 2621440 | tf_op jit(solution)/shard_map/reduce_scatter | solution.py:122
  26.3 30.9 %collective-permute-start.1 = (bf16[1024,128]{0,1:T(8,128)(2,1)S(1)}, bf16[1024,128]{0,1:T(8,128)(2,1)S(1)}, u32[]{:S(2)}, u32[]{:S(2)}) collective-permute-start(bf16[1024,128]{0,1:T(8,128)(2,1)S(1)} %maximum_select_fusion.2), channel_id=1, source_target_pairs={{0,8},{4,12},{8,0},{12,4},{16,24},{20,28},{24,16},{28,20},{1,9},{5... | collective-permute-start | bytes 786440 | tf_op jit(solution)/shard_map/ppermute | solution.py:15
  57.2 5.0 %copy-start.1 = (bf16[2048,128]{0,1:T(8,128)(2,1)}, bf16[2048,128]{0,1:T(8,128)(2,1)S(1)}, u32[]{:S(2)}) copy-start(bf16[2048,128]{0,1:T(8,128)(2,1)S(1)} %maximum_select_fusion.1) | copy-start | bytes 1572868
  57.3 27.9 %collective-permute-start.2 = (bf16[2048,128]{0,1:T(8,128)(2,1)S(1)}, bf16[2048,128]{0,1:T(8,128)(2,1)}, u32[]{:S(2)}, u32[]{:S(2)}) collective-permute-start(bf16[2048,128]{0,1:T(8,128)(2,1)S(1)} %maximum_select_fusion.1), channel_id=1, source_target_pairs={{0,16},{4,20},{8,24},{12,28},{16,0},{20,4},{24,8},{28,12},{1,17},{... | collective-permute-start | bytes 1572872 | tf_op jit(solution)/shard_map/ppermute | solution.py:15
  144.2 60.9 %reduce-scatter.5.cloned.1.call-start = ((), (), s32[]{:S(2)}) async-start(), calls=%async_computation.5 | async-start | bytes 1966080 | tf_op jit(solution)/shard_map/reduce_scatter | solution.py:149
  144.4 4.6 %copy-start.8 = (bf16[1,2048,1024]{2,1,0:T(8,128)(2,1)S(1)}, bf16[1,2048,1024]{2,1,0:T(8,128)(2,1)}, u32[]{:S(2)}) copy-start(bf16[1,2048,1024]{2,1,0:T(8,128)(2,1)} %param.28) | copy-start | bytes 12582916
  149.0 3.7 %copy-start.9 = (bf16[1,1024,2048]{2,1,0:T(8,128)(2,1)S(1)}, bf16[1,1024,2048]{2,1,0:T(8,128)(2,1)}, u32[]{:S(2)}) copy-start(bf16[1,1024,2048]{2,1,0:T(8,128)(2,1)} %param.29) | copy-start | bytes 12582916
  152.7 3.0 %copy-start.4 = (f32[128,2]{0,1:T(2,128)S(1)}, f32[128,2]{0,1:T(2,128)}, u32[]{:S(2)}) copy-start(f32[128,2]{0,1:T(2,128)} %param.25) | copy-start | bytes 3076
  155.7 54.9 %copy-start.6 = (f32[2048]{0:T(1024)S(1)}, f32[2048]{0:T(1024)}, u32[]{:S(2)}) copy-start(f32[2048]{0:T(1024)} %param.22) | copy-start | bytes 24580
  205.1 17.1 %all-to-all-start.1 = ((bf16[8,48,512]{2,1,0:T(8,128)(2,1)}), bf16[8,48,512]{2,1,0:T(8,128)(2,1)S(1)}, u32[]{:S(2)}, u32[]{:S(2)}) async-start(bf16[8,48,512]{2,1,0:T(8,128)(2,1)} %reduce-scatter.5.cloned.1.call-done), calls=%async_computation.3 | async-start | bytes 786432 | tf_op jit(solution)/shard_map/all_to_all | solution.py:152
Sparse Core Ops, SparseCore 0:
  144.3 30.2 reduce-scatter.2
  177.1 27.9 reduce-scatter.4
